TPU v7x, 32 devices: a whole 2x2x4 slice. The times are simulated.
32 devices in a mesh: rep: 2 (over x), fs: 8 (over z, y), tp: 2 (over core).
Axes of the slice: x: 2, y: 2, z: 4, core: 2. Of those that a mesh axis runs over, the one named last changes fastest.
Arguments:
- hidden_in: bfloat16 [12288, 2048], P(('rep', 'fs', 'tp')), may hold values from -6 to 6
- norm_gain: float32 [2048], replicated, may hold values from 0.1 to 1.9
- up_weight: float32 [2048, 8192], P('fs', 'tp'), may hold values from -0.125 to 0.125
- up_scale: float32 [8192], P('tp'), may hold values from 0.5 to 2
- down_weight: float32 [8192, 2048], P('tp', 'fs'), may hold values from -0.0625 to 0.0625
- down_scale: float32 [2048], replicated, may hold values from 0.5 to 2
Outputs:
- layer_out: bfloat16 [12288, 2048], P(('rep', 'fs', 'tp'))
All inputs are finite; a program needn't handle non-finite values.
Results may differ from a plain program's by a relative error of at most 0.0085.
Values may be sent and summed in bfloat16 or wider, within the bound.
A program may use at most 128 MiB of HBM per device.

v0:
```python
import functools

import jax
import jax.numpy as jnp
from jax import lax
from jax.experimental import pallas as pl
from jax.experimental.pallas import tpu as pltpu
from jax.sharding import Mesh, PartitionSpec as P

MESH = pl.DeviceIdType.MESH
LOW = jnp.bfloat16


def kernel(
    n, hidden, gain, up_f32, up_scale, dn_f32, dn_scale, out,
    hid, up_st, dn_st, up_peer, dn_peer,
    tok, up_w, dn_w, act, psend, precv, csum, ra1, rb1, ra2, rb2,
    up_rs, up_sr, up_sl, dn_rs, dn_sr, dn_sl, ss, rs, ls,
):
    x, z, y, c = (lax.axis_index(a) for a in ("rep", "fz", "fy", "tp"))
    ox, oy, oc = 1 - x, 1 - y, 1 - c
    to_x, to_y, to_c = {"rep": ox}, {"fy": oy}, {"tp": oc}
    to_right = {"fz": jnp.minimum(z + 1, n - 1)}
    to_left = {"fz": jnp.maximum(z - 1, 0)}
    has_right, has_left = z < n - 1, z > 0
    tiles, kr, tile = up_peer.shape
    nsub, width, pc = dn_peer.shape
    rows, depth = hid.shape
    cols = nsub * pc
    steps = n * nsub
    top = max(rows // 48, 1) * 16

    def quarter(yy):
        return pl.ds(pl.multiple_of((x * 2 + yy) * width, width), width)

    loads = [
        pltpu.make_async_copy(up_f32.at[:, quarter(y)], up_st.at[0], ls.at[0]),
        pltpu.make_async_copy(up_f32.at[:, quarter(oy)], up_st.at[1], ls.at[1]),
        pltpu.make_async_copy(hidden, hid, ls.at[2]),
        pltpu.make_async_copy(dn_f32.at[quarter(y)], dn_st.at[0], ls.at[3]),
        pltpu.make_async_copy(dn_f32.at[quarter(oy)], dn_st.at[1], ls.at[4]),
    ]
    barrier = pltpu.get_barrier_semaphore()
    for other in (to_x, to_y, to_c):
        pl.semaphore_signal(barrier, inc=1, device_id=other, device_id_type=MESH)

    @pl.when(has_right)
    def _():
        pl.semaphore_signal(barrier, inc=1, device_id=to_right, device_id_type=MESH)

    @pl.when(has_left)
    def _():
        pl.semaphore_signal(barrier, inc=1, device_id=to_left, device_id_type=MESH)

    for copy in loads:
        copy.start()
    here = pl.ds(pl.multiple_of((z * 2 + y) * kr, kr), kr)
    loads[0].wait()
    for j in range(tiles):
        up_w[j, here] = up_st[0, :, j * tile:(j + 1) * tile].astype(LOW)
    loads[1].wait()
    for j in range(tiles):
        up_peer[j] = up_st[1, :, j * tile:(j + 1) * tile].astype(LOW)
    pl.semaphore_wait(barrier, 3 + jnp.minimum(z, 1) + jnp.minimum(n - 1 - z, 1))

    count = [0]
    sent = []

    def remote(src, dst, send_sem, recv_sem, other):
        return pltpu.make_async_remote_copy(
            src_ref=src, dst_ref=dst, send_sem=send_sem, recv_sem=recv_sem,
            device_id=other, device_id_type=MESH,
        )

    def send(src, dst, other):
        i = count[0]
        count[0] += 1
        copy = remote(src, dst, ss.at[i], rs.at[i], other)
        copy.start()
        sent.append(copy)
        return copy

    def up_piece(j, o, yy, right):
        shard = o * 2 + yy
        ref = up_w.at[j, pl.ds(pl.multiple_of(shard * kr, kr), kr)]
        sems = up_sr if right else up_sl
        return remote(ref, ref, sems.at[j, shard], up_rs.at[j, shard], to_right if right else to_left)

    def dn_piece(u, o, yy, right):
        ref = dn_w.at[o, u, yy]
        sems = dn_sr if right else dn_sl
        return remote(
            ref, ref, sems.at[u, o * 2 + yy], dn_rs.at[u, o * 2 + yy], to_right if right else to_left
        )

    def own_pieces(piece, i, yy):
        @pl.when(has_right)
        def _():
            piece(i, z, yy, True).start()

        @pl.when(has_left)
        def _():
            piece(i, z, yy, False).start()

    def ends(t):
        return jnp.maximum(z - t, 0), jnp.minimum(z + t, n - 1)

    def pass_on(piece, i, t):
        before, after = ends(t)

        @pl.when(z - t >= 0)
        def _():
            for yy in (y, oy):
                piece(i, before, yy, True).wait_recv()

                @pl.when(has_right)
                def _():
                    piece(i, before, yy, True).start()

        @pl.when(z + t < n)
        def _():
            for yy in (y, oy):
                piece(i, after, yy, False).wait_recv()

                @pl.when(has_left)
                def _():
                    piece(i, after, yy, False).start()

    def all_sent(piece, i):
        @pl.loop(0, n)
        def _(t):
            before, after = ends(t)
            for yy in (y, oy):
                @pl.when(jnp.logical_and(z - t >= 0, has_right))
                def _():
                    piece(i, before, yy, True).wait_send()

                @pl.when(jnp.logical_and(z + t < n, has_left))
                def _():
                    piece(i, after, yy, False).wait_send()

    own_pieces(up_piece, 0, y)
    y_up = [send(up_peer.at[j], up_w.at[j, here], to_y) for j in range(tiles)]

    loads[2].wait()
    block = min(64, rows)

    @pl.loop(0, rows // block)
    def _(i):
        at = pl.ds(pl.multiple_of(i * block, block), block)
        wide = hid[at].astype(jnp.float32)
        scale = lax.rsqrt(jnp.mean(wide * wide, axis=1, keepdims=True) + 1e-06)
        tok[x, y, c, at] = (wide * scale * gain[...]).astype(LOW)

    loads[3].wait()
    for u in range(nsub):
        dn_w[z, u, y] = dn_st[0, :, u * pc:(u + 1) * pc].astype(LOW)
    loads[4].wait()
    for u in range(nsub):
        dn_peer[u] = dn_st[1, :, u * pc:(u + 1) * pc].astype(LOW)

    def token_part(xx, yy, first):
        return tok.at[xx, yy, c, pl.ds(0, top) if first else pl.ds(top, rows - top)]

    tx = [send(token_part(x, y, f), token_part(x, y, f), to_x) for f in (True, False)]
    ty = [send(token_part(x, y, f), token_part(x, y, f), to_y) for f in (False, True)]
    tc = send(tok.at[x, y, c], tok.at[x, y, c], to_c)

    def own_up(j):
        own_pieces(up_piece, j, y)

    def peer_up(j):
        y_up[j].wait_recv()
        own_pieces(up_piece, j, oy)

    def up_unit(gx, gy, j):
        at = pl.ds(pl.multiple_of(j * tile, tile), tile)
        sc_at = pl.ds(pl.multiple_of((x * 2 + y) * width + j * tile, tile), tile)
        pre = jnp.dot(
            tok[gx, gy].reshape(2 * rows, depth), up_w[j], preferred_element_type=jnp.float32
        )
        value = jnp.square(jnp.maximum(pre * up_scale[:, sc_at], 0.0)).astype(LOW)
        act[0, gx, gy, :, at] = value[:rows]
        act[1, gx, gy, :, at] = value[rows:]

    peer_up(0)
    if tiles > 1:
        own_up(1)
        peer_up(1)

    late = {}
    for j in range(tiles):
        last = j == tiles - 1
        if 2 <= j + 1 < tiles:
            own_up(j + 1)
            peer_up(j + 1)
        if last:
            own_pieces(dn_piece, 0, y)
        for t in range(1, n):
            pass_on(up_piece, j, t)
            if j == 0 and t == n - 1:
                tx[0].wait_recv()
                late["diag_y"] = send(token_part(ox, y, True), token_part(ox, y, True), to_y)
                late["y_dn"] = [send(dn_peer.at[u], dn_w.at[z, u, y], to_y) for u in range(nsub)]
            if j == tiles // 2 - 1 and t == n - 1:
                ty[0].wait_recv()
                late["diag_x"] = send(token_part(x, oy, False), token_part(x, oy, False), to_x)
                tx[1].wait_recv()
                cx = send(tok.at[ox, y, c], tok.at[ox, y, c], to_c)
            if j == tiles - 2:
                if t == max(1, n // 3):
                    tc.wait_recv()
                    cx.wait_recv()

                    @pl.loop(0, 2 * (tiles - 2))
                    def _(i):
                        g = i % 2
                        up_unit(x + g * (ox - x), y, i // 2)
                if t == max(1, (2 * n) // 3):
                    ty[1].wait_recv()
                    cy = send(tok.at[x, oy, c], tok.at[x, oy, c], to_c)
            if last:
                if t == 1:
                    cy.wait_recv()

                    @pl.loop(0, tiles - 1)
                    def _(i):
                        up_unit(x, oy, i)
                if t == max(1, n // 3):
                    late["diag_y"].wait_recv()
                    late["diag_x"].wait_recv()
                    cd = send(tok.at[ox, oy, c], tok.at[ox, oy, c], to_c)

                    @pl.loop(0, 2)
                    def _(g):
                        up_unit(x + g * (ox - x), y, tiles - 2)
                if t == max(1, (2 * n) // 3):
                    cd.wait_recv()

                    @pl.loop(0, tiles - 1)
                    def _(i):
                        up_unit(ox, oy, i)
    late["y_dn"][0].wait_recv()
    own_pieces(dn_piece, 0, oy)
    for u in range(1, nsub):
        own_pieces(dn_piece, u, y)
        late["y_dn"][u].wait_recv()
        own_pieces(dn_piece, u, oy)

    @pl.loop(0, 4)
    def _(i):
        up_unit(i // 2, i % 2, tiles - 1)

    side = jnp.minimum(z, n - 1 - z)
    far = jnp.where(z <= n - 1 - z, 1, -1)

    def owner(s):
        p = s // nsub
        near = z + (-1 if p % 2 else 1) * ((p + 1) // 2)
        return jnp.where(p <= 2 * side, near, z + far * (p - side))

    def each_part(s, cc, emit):
        o, u = owner(s), s % nsub

        @pl.loop(0, 2)
        def _(xx):
            left = act[cc, xx].reshape(2 * rows, width)
            if pc % 128 == 0:
                right = jnp.concatenate([dn_w[o, u, 0], dn_w[o, u, 1]], axis=1)
                both = jnp.dot(left, right, preferred_element_type=jnp.float32)
                halves = both[:, :pc], both[:, pc:]
            else:
                halves = [
                    jnp.dot(left, dn_w[o, u, yy], preferred_element_type=jnp.float32)
                    for yy in range(2)
                ]
            for yy in range(2):
                at = slice(yy * rows, (yy + 1) * rows)
                emit(0, xx, yy, halves[0][at].astype(LOW))
                emit(1, yy, xx, halves[1][at].astype(LOW))

    given, first, second = {}, {}, {}

    def for_partner(s):
        p = s % 2
        if s >= 2:
            given[s - 2].wait_send()

        def emit(h, f, g, part):
            psend[p, h, f, g] = part

        each_part(s, oc, emit)
        given[s] = send(psend.at[p], precv.at[s], to_c)

    def for_own(s):
        p = s % 2

        def emit(h, f, g, part):
            csum[p, h, f, g] = part

        each_part(s, c, emit)
        given[s].wait_recv()
        total = csum[p].astype(jnp.float32) + precv[s].astype(jnp.float32)
        csum[p] = total.astype(LOW)
        first[s] = (
            send(csum.at[p, 0, ox], ra1.at[s], to_x),
            send(csum.at[p, 1, oy], rb1.at[s], to_y),
        )

    def second_stage(s):
        p = s % 2
        pair = []
        for h, f, g, got, dst, other in (
            (0, x, oy, ra1, ra2, to_y), (1, y, ox, rb1, rb2, to_x)
        ):
            first[s][h].wait_recv()
            total = csum[p, h, f, g].astype(jnp.float32) + got[s, g].astype(jnp.float32)
            csum[p, h, f, g] = total.astype(LOW)
            pair.append(send(csum.at[p, h, f, g], dst.at[s], other))
        second[s] = pair

    def finish(s):
        p = s % 2
        o, u = owner(s), s % nsub
        for h, f, g, one, two in ((0, x, y, ra1, ra2), (1, y, x, rb1, rb2)):
            second[s][h].wait_recv()
            total = csum[p, h, f, g].astype(jnp.float32) + one[s, g].astype(jnp.float32)
            total = total + two[s].astype(jnp.float32)
            slot = (o * 2 + h) * nsub + u
            if pc % 128 == 0:
                at = pl.ds(pl.multiple_of(slot * pc, pc), pc)
                out[:, at] = (total * dn_scale[:, at]).astype(out.dtype)
            else:
                out[slot] = (total * dn_scale[slot]).astype(out.dtype)
        for copy in (*first[s], *second[s]):
            copy.wait_send()

    for s in range(steps):
        for_partner(s)
        if s >= 2:
            finish(s - 2)
        for_own(s)
        second_stage(s)
        e = s - nsub + 1
        if 0 <= e < (n - 1) * nsub:
            pass_on(dn_piece, e % nsub, e // nsub + 1)
    finish(steps - 2)
    finish(steps - 1)
    for j in range(tiles):
        all_sent(up_piece, j)
    for u in range(nsub):
        all_sent(dn_piece, u)
    for copy in (
        *y_up, *tx, *ty, tc, late["diag_y"], *late["y_dn"], late["diag_x"], cx, cy, cd,
        given[steps - 2], given[steps - 1],
    ):
        copy.wait_send()


def body(hidden_in, norm_gain, up_weight, up_scale, down_weight, down_scale):
    n = lax.axis_size("fz")
    rows, depth = hidden_in.shape
    kr, cols = up_weight.shape[0], down_weight.shape[1]
    width = up_weight.shape[1] // 4
    tile = min(256, width)
    tiles = width // tile
    pc = min(128, cols)
    nsub = cols // pc
    steps = n * nsub
    flat = pc % 128 == 0
    sends = tiles + 10 + nsub + 5 * steps
    vmem = pl.BlockSpec(memory_space=pltpu.VMEM)
    hbm = pl.BlockSpec(memory_space=pl.ANY)
    dma = pltpu.SemaphoreType.DMA
    made = pl.pallas_call(
        functools.partial(kernel, n),
        out_shape=jax.ShapeDtypeStruct((rows, depth) if flat else (2 * steps, rows, pc), LOW),
        in_specs=[hbm, vmem, hbm, vmem, hbm, vmem],
        out_specs=vmem,
        scratch_shapes=[
            pltpu.VMEM((rows, depth), LOW),
            pltpu.VMEM((2, kr, width), jnp.float32),
            pltpu.VMEM((2, width, cols), jnp.float32),
            pltpu.VMEM((tiles, kr, tile), LOW),
            pltpu.VMEM((nsub, width, pc), LOW),
            pltpu.VMEM((2, 2, 2, rows, depth), LOW),
            pltpu.VMEM((tiles, depth, tile), LOW),
            pltpu.VMEM((n, nsub, 2, width, pc), LOW),
            pltpu.VMEM((2, 2, 2, rows, width), LOW),
            pltpu.VMEM((2, 2, 2, 2, rows, pc), LOW),
            pltpu.VMEM((steps, 2, 2, 2, rows, pc), LOW),
            pltpu.VMEM((2, 2, 2, 2, rows, pc), LOW),
            pltpu.VMEM((steps, 2, rows, pc), LOW),
            pltpu.VMEM((steps, 2, rows, pc), LOW),
            pltpu.VMEM((steps, rows, pc), LOW),
            pltpu.VMEM((steps, rows, pc), LOW),
            dma((tiles, 2 * n)), dma((tiles, 2 * n)), dma((tiles, 2 * n)),
            dma((nsub, 2 * n)), dma((nsub, 2 * n)), dma((nsub, 2 * n)),
            dma((sends,)), dma((sends,)), dma((5,)),
        ],
        compiler_params=pltpu.CompilerParams(
            collective_id=0, has_side_effects=True, vmem_limit_bytes=64000 * 1024
        ),
    )(
        hidden_in,
        norm_gain.reshape(1, depth),
        up_weight,
        up_scale.reshape(1, 4 * width),
        down_weight,
        down_scale.reshape((1, depth) if flat else (2 * steps, 1, pc)),
    )
    return made if flat else made.transpose(1, 0, 2).reshape(rows, depth)


def solution(mesh):
    n_rep, n_fs, n_tp = (mesh.shape[a] for a in ("rep", "fs", "tp"))
    split = Mesh(mesh.devices.reshape(n_rep, n_fs // 2, 2, n_tp), ("rep", "fz", "fy", "tp"))
    fs = ("fz", "fy")
    tokens = P(("rep", *fs, "tp"), None)
    placed = (tokens, P(), P(fs, "tp"), P("tp"), P("tp", fs), P())
    return jax.shard_map(body, mesh=split, in_specs=placed, out_specs=tokens, check_vma=False)
```

profile of v0, /device:TPU:0, one launch (start us, length us, event | category | flops | bytes accessed | tf_op | source)
XLA Modules:
  0.0 174.0 jit_solution(12989069347021636821)
XLA Ops:
  0.0 171.2 %shard_map.64 = bf16[384,2048]{1,0:T(8,128)(2,1)} custom-call(bf16[384,2048]{1,0:T(8,128)(2,1)} %hidden.1, f32[1,2048]{1,0:T(1,128)} %bitcast.4, f32[256,4096]{1,0:T(8,128)} %up_f32.1, f32[1,4096]{1,0:T(1,128)} %bitcast.3, f32[4096,256]{1,0:T(8,128)} %dn_f32.1, f32[1,2048]{1,0:T(1,128)} %bitcast.5), custom_call_target="tpu_custom_call" | custom-call | tf_op jit(solution)/shard_map/pallas_call | solution.py:375
  171.2 2.7 %copy.8 = bf16[384,2048]{1,0:T(8,128)(2,1)} copy(bf16[384,2048]{1,0:T(8,128)(2,1)} %shard_map.64) | data formatting | bytes 3145728
where the time goes:
time: 174 us
  Pallas kernels  171 us (98%)
  local copies, waits for them, and re-layouts  2.73 us (2%)
    pallas_call x1, Pallas kernels, body(): pl.pallas_call(functools.partial(kernel, n), out_shape=jax.ShapeDtypeStru...  171 us

commit v1 on v0

--- a/solution.py
+++ b/solution.py
@@ -292,8 +292,10 @@
         each_part(s, oc, emit)
         given[s] = send(psend.at[p], precv.at[s], to_c)
 
+    slots = csum.shape[0]
+
     def for_own(s):
-        p = s % 2
+        p = s % slots
 
         def emit(h, f, g, part):
             csum[p, h, f, g] = part
@@ -308,7 +310,7 @@
         )
 
     def second_stage(s):
-        p = s % 2
+        p = s % slots
         pair = []
         for h, f, g, got, dst, other in (
             (0, x, oy, ra1, ra2, to_y), (1, y, ox, rb1, rb2, to_x)
@@ -320,7 +322,7 @@
         second[s] = pair
 
     def finish(s):
-        p = s % 2
+        p = s % slots
         o, u = owner(s), s % nsub
         for h, f, g, one, two in ((0, x, y, ra1, ra2), (1, y, x, rb1, rb2)):
             second[s][h].wait_recv()
@@ -337,13 +339,17 @@
 
     for s in range(steps):
         for_partner(s)
+        for_own(s)
+        if 1 <= s < steps - 1:
+            second_stage(s - 1)
         if s >= 2:
             finish(s - 2)
-        for_own(s)
-        second_stage(s)
+        if s == steps - 2:
+            second_stage(s)
         e = s - nsub + 1
         if 0 <= e < (n - 1) * nsub:
             pass_on(dn_piece, e % nsub, e // nsub + 1)
+    second_stage(steps - 1)
     finish(steps - 2)
     finish(steps - 1)
     for j in range(tiles):
@@ -374,7 +380,7 @@
     dma = pltpu.SemaphoreType.DMA
     made = pl.pallas_call(
         functools.partial(kernel, n),
-        out_shape=jax.ShapeDtypeStruct((rows, depth) if flat else (2 * steps, rows, pc), LOW),
+        out_shape=pltpu.VMEM((rows, depth), LOW) if flat else jax.ShapeDtypeStruct((2 * steps, rows, pc), LOW),
         in_specs=[hbm, vmem, hbm, vmem, hbm, vmem],
         out_specs=vmem,
         scratch_shapes=[
@@ -389,7 +395,7 @@
             pltpu.VMEM((2, 2, 2, rows, width), LOW),
             pltpu.VMEM((2, 2, 2, 2, rows, pc), LOW),
             pltpu.VMEM((steps, 2, 2, 2, rows, pc), LOW),
-            pltpu.VMEM((2, 2, 2, 2, rows, pc), LOW),
+            pltpu.VMEM((3, 2, 2, 2, rows, pc), LOW),
             pltpu.VMEM((steps, 2, rows, pc), LOW),
             pltpu.VMEM((steps, 2, rows, pc), LOW),
             pltpu.VMEM((steps, rows, pc), LOW),
@@ -399,7 +405,7 @@
             dma((sends,)), dma((sends,)), dma((5,)),
         ],
         compiler_params=pltpu.CompilerParams(
-            collective_id=0, has_side_effects=True, vmem_limit_bytes=64000 * 1024
+            collective_id=0, has_side_effects=True, vmem_limit_bytes=(56000 if flat else 64000) * 1024
         ),
     )(
         hidden_in,

time: 174 us -> 161 us (0.925)
  Pallas kernels: 171 us -> 160 us
    pallas_call x1, Pallas kernels: 171 us -> 160 us  [body(): pl.pallas_call(functools.partial(kernel, n), out_shape=pltpu.VMEM((rows,...]
where the time goes in v1:
time: 161 us
  Pallas kernels  160 us (99%)
    pallas_call x1, Pallas kernels, body(): pl.pallas_call(functools.partial(kernel, n), out_shape=pltpu.VMEM((rows,...  160 us

profile of v1, /device:TPU:0, one launch (start us, length us, event | category | flops | bytes accessed | tf_op | source)
XLA Modules:
  0.0 160.8 jit_solution(3188856784671166758)
XLA Ops:
  0.0 159.6 %shard_map.64 = bf16[384,2048]{1,0:T(8,128)(2,1)S(1)} custom-call(bf16[384,2048]{1,0:T(8,128)(2,1)} %hidden.1, f32[1,2048]{1,0:T(1,128)} %bitcast.4, f32[256,4096]{1,0:T(8,128)} %up_f32.1, f32[1,4096]{1,0:T(1,128)} %bitcast.3, f32[4096,256]{1,0:T(8,128)} %dn_f32.1, f32[1,2048]{1,0:T(1,128)} %bitcast.5), custom_call_target="tpu_custom_call" | custom-call | tf_op jit(solution)/shard_map/pallas_call | solution.py:381
  159.6 1.1 copy.8

commit v2 on v1

--- a/solution.py
+++ b/solution.py
@@ -12,8 +12,8 @@
 
 
 def kernel(
-    n, hidden, gain, up_f32, up_scale, dn_f32, dn_scale, out,
-    hid, up_st, dn_st, up_peer, dn_peer,
+    n, hidden, gain_in, up_f32, up_scale_in, dn_f32, dn_scale_in, out,
+    gain, up_scale, dn_scale, hid, up_st, dn_st, up_peer, dn_peer,
     tok, up_w, dn_w, act, psend, precv, csum, ra1, rb1, ra2, rb2,
     up_rs, up_sr, up_sl, dn_rs, dn_sr, dn_sl, ss, rs, ls,
 ):
@@ -26,20 +26,31 @@
     tiles, kr, tile = up_peer.shape
     nsub, width, pc = dn_peer.shape
     rows, depth = hid.shape
-    cols = nsub * pc
-    steps = n * nsub
     top = max(rows // 48, 1) * 16
 
     def quarter(yy):
         return pl.ds(pl.multiple_of((x * 2 + yy) * width, width), width)
 
+    def up_load(yy, side, lo, hi, sem):
+        start = (x * 2 + yy) * width + lo
+        return pltpu.make_async_copy(
+            up_f32.at[:, pl.ds(pl.multiple_of(start, tile), hi - lo)],
+            up_st.at[side, :, pl.ds(lo, hi - lo)], sem,
+        )
+
     loads = [
-        pltpu.make_async_copy(up_f32.at[:, quarter(y)], up_st.at[0], ls.at[0]),
-        pltpu.make_async_copy(up_f32.at[:, quarter(oy)], up_st.at[1], ls.at[1]),
+        up_load(y, 0, 0, tile, ls.at[0]),
+        up_load(oy, 1, 0, tile, ls.at[1]),
         pltpu.make_async_copy(hidden, hid, ls.at[2]),
-        pltpu.make_async_copy(dn_f32.at[quarter(y)], dn_st.at[0], ls.at[3]),
-        pltpu.make_async_copy(dn_f32.at[quarter(oy)], dn_st.at[1], ls.at[4]),
+        up_load(y, 0, tile, width, ls.at[3]),
+        up_load(oy, 1, tile, width, ls.at[4]),
+        pltpu.make_async_copy(dn_f32.at[quarter(y)], dn_st.at[0], ls.at[5]),
+        pltpu.make_async_copy(dn_f32.at[quarter(oy)], dn_st.at[1], ls.at[6]),
+        pltpu.make_async_copy(gain_in, gain, ls.at[7]),
+        pltpu.make_async_copy(up_scale_in.at[:, quarter(y)], up_scale, ls.at[8]),
+        pltpu.make_async_copy(dn_scale_in, dn_scale, ls.at[9]),
     ]
+    loads[0].start()
     barrier = pltpu.get_barrier_semaphore()
     for other in (to_x, to_y, to_c):
         pl.semaphore_signal(barrier, inc=1, device_id=other, device_id_type=MESH)
@@ -52,15 +63,22 @@
     def _():
         pl.semaphore_signal(barrier, inc=1, device_id=to_left, device_id_type=MESH)
 
-    for copy in loads:
+    for copy in loads[1:]:
         copy.start()
     here = pl.ds(pl.multiple_of((z * 2 + y) * kr, kr), kr)
+
+    def low_up(side, tile_range):
+        for j in tile_range:
+            value = up_st[side, :, j * tile:(j + 1) * tile].astype(LOW)
+            if side == 0:
+                up_w[j, here] = value
+            else:
+                up_peer[j] = value
+
     loads[0].wait()
-    for j in range(tiles):
-        up_w[j, here] = up_st[0, :, j * tile:(j + 1) * tile].astype(LOW)
+    low_up(0, range(1))
     loads[1].wait()
-    for j in range(tiles):
-        up_peer[j] = up_st[1, :, j * tile:(j + 1) * tile].astype(LOW)
+    low_up(1, range(1))
     pl.semaphore_wait(barrier, 3 + jnp.minimum(z, 1) + jnp.minimum(n - 1 - z, 1))
 
     count = [0]
@@ -105,12 +123,12 @@
     def ends(t):
         return jnp.maximum(z - t, 0), jnp.minimum(z + t, n - 1)
 
-    def pass_on(piece, i, t):
+    def pass_on(piece, i, t, shards):
         before, after = ends(t)
 
         @pl.when(z - t >= 0)
         def _():
-            for yy in (y, oy):
+            for yy in shards:
                 piece(i, before, yy, True).wait_recv()
 
                 @pl.when(has_right)
@@ -119,7 +137,7 @@
 
         @pl.when(z + t < n)
         def _():
-            for yy in (y, oy):
+            for yy in shards:
                 piece(i, after, yy, False).wait_recv()
 
                 @pl.when(has_left)
@@ -139,10 +157,18 @@
                 def _():
                     piece(i, after, yy, False).wait_send()
 
+    def send_peer(j):
+        return send(up_peer.at[j], up_w.at[j, here], to_y)
+
     own_pieces(up_piece, 0, y)
-    y_up = [send(up_peer.at[j], up_w.at[j, here], to_y) for j in range(tiles)]
-
+    y_up = [send_peer(0)]
+    loads[3].wait()
+    low_up(0, range(1, tiles))
+    loads[4].wait()
+    low_up(1, range(1, tiles))
     loads[2].wait()
+    loads[7].wait()
+    y_up += [send_peer(j) for j in range(1, tiles)]
     block = min(64, rows)
 
     @pl.loop(0, rows // block)
@@ -152,12 +178,15 @@
         scale = lax.rsqrt(jnp.mean(wide * wide, axis=1, keepdims=True) + 1e-06)
         tok[x, y, c, at] = (wide * scale * gain[...]).astype(LOW)
 
-    loads[3].wait()
+    loads[5].wait()
     for u in range(nsub):
         dn_w[z, u, y] = dn_st[0, :, u * pc:(u + 1) * pc].astype(LOW)
-    loads[4].wait()
+    loads[6].wait()
     for u in range(nsub):
         dn_peer[u] = dn_st[1, :, u * pc:(u + 1) * pc].astype(LOW)
+
+    loads[8].wait()
+    loads[9].wait()
 
     def token_part(xx, yy, first):
         return tok.at[xx, yy, c, pl.ds(0, top) if first else pl.ds(top, rows - top)]
@@ -175,11 +204,10 @@
 
     def up_unit(gx, gy, j):
         at = pl.ds(pl.multiple_of(j * tile, tile), tile)
-        sc_at = pl.ds(pl.multiple_of((x * 2 + y) * width + j * tile, tile), tile)
         pre = jnp.dot(
             tok[gx, gy].reshape(2 * rows, depth), up_w[j], preferred_element_type=jnp.float32
         )
-        value = jnp.square(jnp.maximum(pre * up_scale[:, sc_at], 0.0)).astype(LOW)
+        value = jnp.square(jnp.maximum(pre * up_scale[:, at], 0.0)).astype(LOW)
         act[0, gx, gy, :, at] = value[:rows]
         act[1, gx, gy, :, at] = value[rows:]
 
@@ -197,7 +225,7 @@
         if last:
             own_pieces(dn_piece, 0, y)
         for t in range(1, n):
-            pass_on(up_piece, j, t)
+            pass_on(up_piece, j, t, (y, oy))
             if j == 0 and t == n - 1:
                 tx[0].wait_recv()
                 late["diag_y"] = send(token_part(ox, y, True), token_part(ox, y, True), to_y)
@@ -253,114 +281,137 @@
 
     side = jnp.minimum(z, n - 1 - z)
     far = jnp.where(z <= n - 1 - z, 1, -1)
-
-    def owner(s):
-        p = s // nsub
+    half = rows // 2
+    plan = [(p, u, None) for p in range(n) for u in range(nsub)]
+    if pc % 128 == 0:
+        plan = plan[:-1] + [(n - 1, nsub - 1, 0), (n - 1, nsub - 1, 1)]
+    steps = len(plan)
+    slots = csum.shape[0]
+
+    def span(s):
+        return pl.ds(0, rows if plan[s][2] is None else half)
+
+    def owner(p):
         near = z + (-1 if p % 2 else 1) * ((p + 1) // 2)
         return jnp.where(p <= 2 * side, near, z + far * (p - side))
 
-    def each_part(s, cc, emit):
-        o, u = owner(s), s % nsub
-
-        @pl.loop(0, 2)
-        def _(xx):
-            left = act[cc, xx].reshape(2 * rows, width)
-            if pc % 128 == 0:
-                right = jnp.concatenate([dn_w[o, u, 0], dn_w[o, u, 1]], axis=1)
-                both = jnp.dot(left, right, preferred_element_type=jnp.float32)
-                halves = both[:, :pc], both[:, pc:]
-            else:
-                halves = [
-                    jnp.dot(left, dn_w[o, u, yy], preferred_element_type=jnp.float32)
-                    for yy in range(2)
-                ]
+    def parts(s, cc, xx, dst):
+        p, u, single = plan[s]
+        o = owner(p)
+        left = act[cc, xx].reshape(2 * rows, width)
+
+        def dot(right):
+            return jnp.dot(left, right, preferred_element_type=jnp.float32)
+
+        if single is not None:
+            one = dot(dn_w[o, u, single])
             for yy in range(2):
-                at = slice(yy * rows, (yy + 1) * rows)
-                emit(0, xx, yy, halves[0][at].astype(LOW))
-                emit(1, yy, xx, halves[1][at].astype(LOW))
+                for h in range(2):
+                    at = yy * rows + h * half
+                    dst[yy, h, pl.ds(0, half)] = one[at:at + half].astype(LOW)
+            return
+        if pc % 128 == 0:
+            both = dot(jnp.concatenate([dn_w[o, u, 0], dn_w[o, u, 1]], axis=1))
+            halves = both[:, :pc], both[:, pc:]
+        else:
+            halves = [dot(dn_w[o, u, yy]) for yy in range(2)]
+        for yy in range(2):
+            for h in range(2):
+                dst[yy, h] = halves[h][yy * rows:(yy + 1) * rows].astype(LOW)
 
     given, first, second = {}, {}, {}
 
     def for_partner(s):
         p = s % 2
         if s >= 2:
-            given[s - 2].wait_send()
-
-        def emit(h, f, g, part):
-            psend[p, h, f, g] = part
-
-        each_part(s, oc, emit)
-        given[s] = send(psend.at[p], precv.at[s], to_c)
-
-    slots = csum.shape[0]
+            for copy in given[s - 2]:
+                copy.wait_send()
+        given[s] = []
+        at = span(s)
+        for i, xx in enumerate((ox, x)):
+            parts(s, oc, xx, psend.at[p, i])
+            given[s].append(
+                send(psend.at[p, i, :, :, at], precv.at[s, i, :, :, at], to_c)
+            )
 
     def for_own(s):
-        p = s % slots
-
-        def emit(h, f, g, part):
-            csum[p, h, f, g] = part
-
-        each_part(s, c, emit)
-        given[s].wait_recv()
-        total = csum[p].astype(jnp.float32) + precv[s].astype(jnp.float32)
-        csum[p] = total.astype(LOW)
-        first[s] = (
-            send(csum.at[p, 0, ox], ra1.at[s], to_x),
-            send(csum.at[p, 1, oy], rb1.at[s], to_y),
-        )
+        p, at = s % slots, span(s)
+
+        def first_send(i, yy, h, dst, k, other):
+            return send(csum.at[p, i, yy, h, at], dst.at[s, k, at], other)
+
+        for i, xx in enumerate((ox, x)):
+            parts(s, c, xx, csum.at[p, i])
+            given[s][i].wait_recv()
+            mine, theirs = csum[p, i, :, :, at], precv[s, i, :, :, at]
+            total = mine.astype(jnp.float32) + theirs.astype(jnp.float32)
+            csum[p, i, :, :, at] = total.astype(LOW)
+            if i == 0:
+                first[s] = [
+                    first_send(0, oy, 0, ra1, 0, to_x),
+                    first_send(0, oy, 1, rb1, 0, to_y),
+                    first_send(0, y, 0, ra1, 1, to_x),
+                ]
+        first[s].append(first_send(1, oy, 1, rb1, 1, to_y))
 
     def second_stage(s):
-        p = s % slots
-        pair = []
-        for h, f, g, got, dst, other in (
-            (0, x, oy, ra1, ra2, to_y), (1, y, ox, rb1, rb2, to_x)
-        ):
+        p, at = s % slots, span(s)
+        second[s] = []
+        for h, i, yy, got, dst, other in ((0, 1, oy, ra1, ra2, to_y), (1, 0, y, rb1, rb2, to_x)):
             first[s][h].wait_recv()
-            total = csum[p, h, f, g].astype(jnp.float32) + got[s, g].astype(jnp.float32)
-            csum[p, h, f, g] = total.astype(LOW)
-            pair.append(send(csum.at[p, h, f, g], dst.at[s], other))
-        second[s] = pair
+            total = csum[p, i, yy, h, at].astype(jnp.float32) + got[s, 0, at].astype(jnp.float32)
+            csum[p, i, yy, h, at] = total.astype(LOW)
+            second[s].append(send(csum.at[p, i, yy, h, at], dst.at[s, at], other))
 
     def finish(s):
-        p = s % slots
-        o, u = owner(s), s % nsub
-        for h, f, g, one, two in ((0, x, y, ra1, ra2), (1, y, x, rb1, rb2)):
+        q, at = s % slots, span(s)
+        p, u, single = plan[s]
+        for h, one, two in ((0, ra1, ra2), (1, rb1, rb2)):
+            first[s][2 + h].wait_recv()
             second[s][h].wait_recv()
-            total = csum[p, h, f, g].astype(jnp.float32) + one[s, g].astype(jnp.float32)
-            total = total + two[s].astype(jnp.float32)
-            slot = (o * 2 + h) * nsub + u
+            total = csum[q, 1, y, h, at].astype(jnp.float32) + one[s, 1, at].astype(jnp.float32)
+            total = total + two[s, at].astype(jnp.float32)
+            slot = (owner(p) * 2 + (h if single is None else single)) * nsub + u
+            put = pl.ds(0, rows) if single is None else pl.ds(h * half, half)
             if pc % 128 == 0:
-                at = pl.ds(pl.multiple_of(slot * pc, pc), pc)
-                out[:, at] = (total * dn_scale[:, at]).astype(out.dtype)
+                to = pl.ds(pl.multiple_of(slot * pc, pc), pc)
+                out[put, to] = (total * dn_scale[:, to]).astype(out.dtype)
             else:
-                out[slot] = (total * dn_scale[slot]).astype(out.dtype)
+                out[slot, put] = (total * dn_scale[slot]).astype(out.dtype)
         for copy in (*first[s], *second[s]):
             copy.wait_send()
 
+    events = [(t, u, (0, 1)) for t in range(1, n) for u in range(nsub)]
+    if pc % 128 == 0:
+        events = events[:-1] + [(n - 1, nsub - 1, (0,)), (n - 1, nsub - 1, (1,))]
     for s in range(steps):
         for_partner(s)
         for_own(s)
-        if 1 <= s < steps - 1:
+        if s >= 1 and s != steps - 2:
             second_stage(s - 1)
         if s >= 2:
             finish(s - 2)
-        if s == steps - 2:
+        if s == steps - 3:
             second_stage(s)
+        if s == 1:
+            for j in range(tiles):
+                all_sent(up_piece, j)
+            for copy in (*y_up, *tx, *ty, tc, cx, cy, cd, *late["y_dn"]):
+                copy.wait_send()
+            late["diag_y"].wait_send()
+            late["diag_x"].wait_send()
         e = s - nsub + 1
-        if 0 <= e < (n - 1) * nsub:
-            pass_on(dn_piece, e % nsub, e // nsub + 1)
+        if 0 <= e < len(events):
+            t, u, shards = events[e]
+            pass_on(dn_piece, u, t, shards)
     second_stage(steps - 1)
     finish(steps - 2)
     finish(steps - 1)
-    for j in range(tiles):
-        all_sent(up_piece, j)
     for u in range(nsub):
         all_sent(dn_piece, u)
-    for copy in (
-        *y_up, *tx, *ty, tc, late["diag_y"], *late["y_dn"], late["diag_x"], cx, cy, cd,
-        given[steps - 2], given[steps - 1],
-    ):
-        copy.wait_send()
+    for s in (steps - 2, steps - 1):
+        for copy in given[s]:
+            copy.wait_send()
 
 
 def body(hidden_in, norm_gain, up_weight, up_scale, down_weight, down_scale):
@@ -372,18 +423,22 @@
     tiles = width // tile
     pc = min(128, cols)
     nsub = cols // pc
-    steps = n * nsub
+    pieces = n * nsub
     flat = pc % 128 == 0
-    sends = tiles + 10 + nsub + 5 * steps
+    steps = pieces + (1 if flat else 0)
+    sends = tiles + 10 + nsub + 8 * steps
     vmem = pl.BlockSpec(memory_space=pltpu.VMEM)
     hbm = pl.BlockSpec(memory_space=pl.ANY)
     dma = pltpu.SemaphoreType.DMA
     made = pl.pallas_call(
         functools.partial(kernel, n),
-        out_shape=pltpu.VMEM((rows, depth), LOW) if flat else jax.ShapeDtypeStruct((2 * steps, rows, pc), LOW),
-        in_specs=[hbm, vmem, hbm, vmem, hbm, vmem],
+        out_shape=pltpu.VMEM((rows, depth), LOW) if flat else jax.ShapeDtypeStruct((2 * pieces, rows, pc), LOW),
+        in_specs=[hbm] * 6,
         out_specs=vmem,
         scratch_shapes=[
+            pltpu.VMEM((1, depth), jnp.float32),
+            pltpu.VMEM((1, width), jnp.float32),
+            pltpu.VMEM((1, depth) if flat else (2 * pieces, 1, pc), jnp.float32),
             pltpu.VMEM((rows, depth), LOW),
             pltpu.VMEM((2, kr, width), jnp.float32),
             pltpu.VMEM((2, width, cols), jnp.float32),
@@ -402,10 +457,10 @@
             pltpu.VMEM((steps, rows, pc), LOW),
             dma((tiles, 2 * n)), dma((tiles, 2 * n)), dma((tiles, 2 * n)),
             dma((nsub, 2 * n)), dma((nsub, 2 * n)), dma((nsub, 2 * n)),
-            dma((sends,)), dma((sends,)), dma((5,)),
+            dma((sends,)), dma((sends,)), dma((10,)),
         ],
         compiler_params=pltpu.CompilerParams(
-            collective_id=0, has_side_effects=True, vmem_limit_bytes=(56000 if flat else 64000) * 1024
+            collective_id=0, has_side_effects=True, vmem_limit_bytes=(57000 if flat else 65400) * 1024
         ),
     )(
         hidden_in,
@@ -413,7 +468,7 @@
         up_weight,
         up_scale.reshape(1, 4 * width),
         down_weight,
-        down_scale.reshape((1, depth) if flat else (2 * steps, 1, pc)),
+        down_scale.reshape((1, depth) if flat else (2 * pieces, 1, pc)),
     )
     return made if flat else made.transpose(1, 0, 2).reshape(rows, depth)
 

time: 161 us -> 159 us (0.988)
  Pallas kernels: 160 us -> 158 us
where the time goes in v2:
time: 159 us
  Pallas kernels  158 us (99%)
    pallas_call x1, Pallas kernels, body(): pl.pallas_call(functools.partial(kernel, n), out_shape=pltpu.VMEM((rows,...  158 us

profile of v2, /device:TPU:0, one launch (start us, length us, event | category | flops | bytes accessed | tf_op | source)
XLA Modules:
  0.0 159.3 jit_solution(4020272418200970842)
XLA Ops:
  0.0 158.2 %shard_map.64 = bf16[384,2048]{1,0:T(8,128)(2,1)S(1)} custom-call(bf16[384,2048]{1,0:T(8,128)(2,1)} %hidden.1, f32[1,2048]{1,0:T(1,128)} %bitcast.4, f32[256,4096]{1,0:T(8,128)} %up_f32.1, f32[1,4096]{1,0:T(1,128)} %bitcast.3, f32[4096,256]{1,0:T(8,128)} %dn_f32.1, f32[1,2048]{1,0:T(1,128)} %bitcast.5), custom_call_target="tpu_custom_call" | custom-call | tf_op jit(solution)/shard_map/pallas_call | solution.py:433
  158.2 1.1 copy.8
